TPU v7x, 512 devices: a whole 4x8x8 slice. The times are simulated.
512 devices in a mesh: sp: 32 (over z, x), tp: 16 (over y, core).
Axes of the slice: x: 4, y: 8, z: 8, core: 2. Of those that a mesh axis runs over, the one named last changes fastest.
Arguments:
- tokens: bfloat16 [16384, 4096], P('sp', 'tp'), may hold values from -8 to 8
- w_key: bfloat16 [4096, 2048], P(None, 'tp'), may hold values from -0.09375 to 0.09375
- w_value: bfloat16 [4096, 2048], P(None, 'tp'), may hold values from -0.09375 to 0.09375
- w_beta: bfloat16 [4096, 16], replicated, may hold values from -0.09375 to 0.09375
- w_decay: bfloat16 [4096, 16], replicated, may hold values from -0.09375 to 0.09375
- beta_bias: float32 [16], replicated, may hold values from -6 to -4
- decay_rate: float32 [16], replicated, as said below
- forgetting_increment: float32 [16, 16384], P('tp', 'sp')
- new_query: bfloat16 [16, 128], P('tp', 'sp'), may hold values from -6 to 6
- read_gain: bfloat16 [128], replicated, may hold values from 0.099609375 to 1.8984375
Outputs:
- state_cache: bfloat16 [16, 128, 128], P('tp', 'sp')
- first_read: float32 [16, 128], P('tp')
Inputs may be any that keep to these rules, and one draw needn't show every extreme that they name: `decay_rate`: positive.
All inputs are finite; a program needn't handle non-finite values.
Results may differ from a plain program's by a relative error of at most 0.0075.
Values may be sent and summed in bfloat16 or wider, within the bound.
A program may use at most 64 MiB of HBM per device.

v0:
```python
import jax
import jax.numpy as jnp
from jax import lax
from jax.sharding import Mesh
from jax.sharding import PartitionSpec as P

DK = 128
DV = 128
BLOCK = 64
SP = ("sp_0", "sp_1")
norm_eps = 1e-06


def neutral_like(x, identity):
    return jnp.zeros_like(x) + jnp.asarray(identity, x.dtype)


def entering(x, axes, combine, identity):
    before = start = neutral_like(x, identity)
    running = x
    for axis in reversed(axes):
        count, mine = (lax.axis_size(axis), lax.axis_index(axis))
        pieces = lax.all_gather(running, axis)
        inside, running = (start, start)
        for k in reversed(range(count)):
            passed = k > mine
            running = combine(running, pieces[k])
            inside = jnp.where(passed, running, inside)
        before = combine(inside, before)
    return before


def cut_along(x, dim, count):
    lengths = x.shape
    pieces = x.reshape(*lengths[:dim], count, lengths[dim] // count, *lengths[dim + 1 :])
    return jnp.moveaxis(pieces, dim, 0)


def summed_on_arrival(x, axis, dim):
    pieces = cut_along(x, dim, lax.axis_size(axis))
    arrived = lax.all_to_all(pieces, axis, split_axis=0, concat_axis=0, tiled=True)
    return arrived.sum(axis=0)


def from_everyone(x, axis):
    count = lax.axis_size(axis)
    return lax.all_to_all(jnp.broadcast_to(x[None], (count, *x.shape)), axis, 0, 0, tiled=True)


def taken_together(x, axis):
    return from_everyone(x, axis).sum(axis=0)


def matmul_f32(left, right):
    return jnp.dot(left, right, precision=lax.Precision.HIGHEST)


def batched_f32(left, right):
    return jnp.einsum("hij,hjk->hik", left, right, precision=lax.Precision.HIGHEST)


def unit_inverse(lower):
    current_size = lower.shape[0]
    identity = jnp.eye(current_size, dtype=jnp.float32)
    result = identity - lower
    lower_power = lower
    covered = 2
    while covered < current_size:
        lower_power = matmul_f32(lower_power, lower_power)
        result = matmul_f32(result, identity + lower_power)
        covered = covered * 2
    return result


def block_terms(key_blk, value_blk, beta_blk, logd_blk):
    current_size = key_blk.shape[0]
    cumulative = jnp.cumsum(logd_blk)
    spread = cumulative[:, None] - cumulative[None, :]
    location_positions = jnp.arange(current_size)
    causal = location_positions[:, None] >= location_positions[None, :]
    strict = location_positions[:, None] > location_positions[None, :]
    decay_table = jnp.where(causal, jnp.exp(jnp.where(causal, spread, 0.0)), 0.0)
    key_beta = key_blk * beta_blk[:, None]
    lower = jnp.where(strict, matmul_f32(key_beta, key_blk.T) * decay_table, 0.0)
    inverse = unit_inverse(lower)
    update = matmul_f32(inverse, value_blk * beta_blk[:, None])
    erase = matmul_f32(inverse, key_beta * jnp.exp(cumulative)[:, None])
    key_remainder = key_blk * jnp.exp(cumulative[-1] - cumulative)[:, None]
    return (update, erase, key_remainder, jnp.exp(cumulative[-1]))


def per_device(
    tokens,
    w_key,
    w_value,
    w_beta,
    w_decay,
    beta_bias,
    decay_rate,
    forgetting_increment,
    new_query,
    read_gain,
):
    heads_here = w_key.shape[1] // DK
    token_count = tokens.shape[0]
    head_start = lax.axis_index("tp") * heads_here
    gate_weights = jnp.concatenate(
        [
            lax.dynamic_slice_in_dim(w_beta, head_start, heads_here, 1),
            lax.dynamic_slice_in_dim(w_decay, head_start, heads_here, 1),
        ],
        axis=1,
    )
    piece = lax.all_gather(tokens, "tp", axis=1, tiled=True)
    key_acc = jnp.dot(piece, w_key, preferred_element_type=jnp.float32)
    value_acc = jnp.dot(piece, w_value, preferred_element_type=jnp.float32)
    gate_acc = jnp.dot(piece, gate_weights, preferred_element_type=jnp.float32)
    key_wide = (
        lax.optimization_barrier(key_acc.astype(jnp.bfloat16))
        .astype(jnp.float32)
        .reshape(token_count, heads_here, DK)
    )
    key_unit = key_wide * lax.rsqrt(jnp.sum(key_wide * key_wide, axis=-1, keepdims=True) + norm_eps)
    value_wide = (
        lax.optimization_barrier(value_acc.astype(jnp.bfloat16))
        .astype(jnp.float32)
        .reshape(token_count, heads_here, DV)
    )
    bias_here = lax.dynamic_slice_in_dim(beta_bias, head_start, heads_here, 0)
    rate_here = lax.dynamic_slice_in_dim(decay_rate, head_start, heads_here, 0)
    beta = jax.nn.sigmoid(gate_acc[:, :heads_here] + bias_here).T
    log_decay = (
        -rate_here[:, None] * jax.nn.softplus(gate_acc[:, heads_here:].T) + forgetting_increment
    )
    blocks = token_count // BLOCK
    key_heads = key_unit.transpose(1, 0, 2).reshape(heads_here, blocks, BLOCK, DK)
    value_heads = value_wide.transpose(1, 0, 2).reshape(heads_here, blocks, BLOCK, DV)
    terms = jax.vmap(jax.vmap(block_terms))(
        key_heads,
        value_heads,
        beta.reshape(heads_here, blocks, BLOCK),
        log_decay.reshape(heads_here, blocks, BLOCK),
    )
    inputs = tuple((jnp.moveaxis(item, 1, 0) for item in terms))
    identity = jnp.broadcast_to(jnp.eye(DK, dtype=jnp.float32), (heads_here, DK, DK))
    value_zeros = jnp.zeros((heads_here, DK, DV), jnp.float32)
    padding = jnp.zeros((heads_here, BLOCK, DK), jnp.float32)

    def advance(state, block_in):
        update, erase, key_remainder, keep = block_in
        fresh = jnp.concatenate([update, padding], axis=-1) - jnp.einsum(
            "hcd,hde->hce", erase, state, precision=lax.Precision.HIGHEST
        )
        state = keep[:, None, None] * state + jnp.einsum(
            "hcd,hce->hde", key_remainder, fresh, precision=lax.Precision.HIGHEST
        )
        return (state, None)

    combined, _ = lax.scan(advance, jnp.concatenate([value_zeros, identity], axis=-1), inputs)
    local_b = combined[:, :, :DV]
    local_left = combined[:, :, DV:]
    later_product = entering(local_left, SP, batched_f32, identity)
    summed = summed_on_arrival(batched_f32(later_product, local_b), SP, 1)
    own_rows = summed.astype(jnp.bfloat16)
    partial_read = jnp.sum(
        new_query.astype(jnp.float32)[:, :, None] * own_rows.astype(jnp.float32), axis=1
    )
    raw_read = taken_together(partial_read, SP)
    first_read = (
        raw_read
        * lax.rsqrt(jnp.mean(raw_read * raw_read, axis=-1, keepdims=True) + norm_eps)
        * read_gain.astype(jnp.float32)
    )
    return (own_rows, first_read)


def solution(mesh):
    finer = Mesh(mesh.devices.reshape(8, 4, mesh.shape["tp"]), ("sp_0", "sp_1", "tp"))
    return jax.shard_map(
        per_device,
        mesh=finer,
        in_specs=(
            P(SP, "tp"),
            P(None, "tp"),
            P(None, "tp"),
            P(),
            P(),
            P(),
            P(),
            P("tp", SP),
            P("tp", SP),
            P(),
        ),
        out_specs=(P("tp", SP, None), P("tp", None)),
        check_vma=False,
    )
```

profile of v0, /device:TPU:8, one launch (start us, length us, event | category | flops | bytes accessed | tf_op | source)
XLA Modules:
  0.0 179.6 jit_solution(8949332273028373998)
XLA Ops:
  7.2 0.7 all-gather.4.cloned.1.call-update
  8.0 1.2 dynamic_slice.26
  9.8 1.3 dynamic_slice.29
  11.2 0.9 constant_dynamic-slice_fusion.1
  12.1 53.6 %all-gather.4.cloned.1.call-done = bf16[512,4096]{1,0:T(8,128)(2,1)} async-done(((bf16[512,256]{1,0:T(8,128)(2,1)}), bf16[512,4096]{1,0:T(8,128)(2,1)}) %all-gather.4.cloned.1.call-update) | async-done | bytes 4194320 | tf_op jit(solution)/shard_map/all_gather | solution.py:114
  65.7 3.5 %convolution_bitcast_fusion.5 = f32[512,2]{0,1:T(2,128)S(1)} fusion(bf16[512,4096]{1,0:T(8,128)(2,1)} %all-gather.4.cloned.1.call-done, bf16[4096,1]{0,1:T(2,128)(2,1)S(1)} %get-tuple-element.81, bf16[4096,1]{0,1:T(2,128)(2,1)S(1)} %get-tuple-element.82), kind=kOutput, calls=%fused_computation.23 | convolution fusion | flops 8421376 | bytes 4214784 | tf_op jit(solution)/shard_map/dot_general | solution.py:117
  69.1 0.7 fusion.77
  70.0 0.2 reduce_window_sum.11
  70.5 3.6 %convolution_convert_fusion.1 = bf16[512,128]{1,0:T(8,128)(2,1)S(1)} fusion(bf16[512,4096]{1,0:T(8,128)(2,1)} %all-gather.4.cloned.1.call-done, bf16[4096,128]{1,0:T(8,128)(2,1)S(1)} %copy-done), kind=kOutput, calls=%fused_computation.20 | convolution fusion | flops 536936448 | bytes 5373952 | tf_op jit(solution)/shard_map/dot_general | solution.py:115
  74.1 1.3 convolution_convert_fusion
  75.7 0.6 fusion.10
  76.3 0.4 fusion.80
  76.7 0.4 fusion.81
  77.0 0.4 fusion.19
  77.5 0.4 fusion.82
  77.8 0.4 fusion.17
  78.2 0.4 fusion.83
  78.6 0.4 fusion.15
  79.0 0.4 convolution_add_fusion
  79.4 0.4 fusion.13
  79.8 0.4 fusion.84
  80.2 0.6 convolution_bitcast_fusion.2
  80.8 0.5 convolution_bitcast_fusion.3
  81.4 14.6 %while.10 = (s32[]{:T(128)}, f32[1,128,256]{2,1,0:T(8,128)S(1)}, f32[8,1]{0,1:T(1,128)S(1)}, f32[8,1,64,128]{3,2,1,0:T(8,128)S(1)}, f32[8,1,64,128]{3,2,1,0:T(8,...) while((s32[]{:T(128)}, f32[1,128,256]{2,1,0:T(8,128)S(1)}, f32[8,1]{0,1:T(1,128)S(1)}, ...), condition=%wide.region_3.4_spmd, body=%wide.region_2.3_spmd.sunk | while | flops 50413568 | bytes 688241 | solution.py:159
  81.4 0.6 constant_dynamic-slice_fusion.4
  82.0 0.2 fusion.132
  82.2 1.0 fusion.133
  83.2 0.6 constant_dynamic-slice_fusion.4
  83.8 0.2 fusion.132
  84.0 1.0 fusion.133
  85.1 0.6 constant_dynamic-slice_fusion.4
  85.7 0.2 fusion.132
  85.9 1.0 fusion.133
  86.9 0.6 constant_dynamic-slice_fusion.4
  87.5 0.2 fusion.132
  87.7 1.0 fusion.133
  88.7 0.6 constant_dynamic-slice_fusion.4
  89.3 0.2 fusion.132
  89.5 1.0 fusion.133
  90.6 0.6 constant_dynamic-slice_fusion.4
  91.2 0.2 fusion.132
  91.4 1.0 fusion.133
  92.4 0.6 constant_dynamic-slice_fusion.4
  93.0 0.2 fusion.132
  93.2 1.0 fusion.133
  94.2 0.6 constant_dynamic-slice_fusion.4
  94.8 0.2 fusion.132
  95.0 1.0 fusion.133
  96.1 12.6 %all-gather = f32[4,128,128]{2,1,0:T(8,128)S(1)} all-gather(f32[1,128,128]{2,1,0:T(8,128)S(1)} %slice.55), channel_id=2, replica_groups=mesh['sp_0'=8,'sp_1'=4,'tp'=16] {'sp_1'}, dimensions={0}, use_global_device_ids=true | all-gather | bytes 327680 | tf_op jit(solution)/shard_map/all_gather | solution.py:23
  108.8 0.2 fusion.58
  109.0 0.2 fusion.57
  109.2 0.2 fusion.56
  109.5 27.6 %all-gather.1 = f32[1024,128]{1,0:T(8,128)S(1)} all-gather(f32[128,128]{1,0:T(8,128)S(1)} %fusion.56), channel_id=3, replica_groups=mesh['sp_0'=8,'sp_1'=4,'tp'=16] {'sp_0'}, dimensions={0}, use_global_device_ids=true | all-gather | bytes 589824 | tf_op jit(solution)/shard_map/all_gather | solution.py:23
  137.2 0.2 fusion.52
  137.4 0.2 fusion.50
  137.9 0.2 fusion.46
  138.7 0.2 convolution_select_fusion
  139.1 0.2 convolution_bitcast_fusion.4
  139.3 0.7 copy.34
  140.0 7.9 %all-to-all-start = ((f32[32,1,4,128]{3,2,1,0:T(4,128)}), f32[32,1,4,128]{3,2,1,0:T(4,128)S(1)}, u32[]{:S(2)}, u32[]{:S(2)}) async-start(f32[32,1,4,128]{3,2,1,0:T(4,128)} %copy.34), calls=%async_computation | async-start | bytes 131072 | tf_op jit(solution)/shard_map/all_to_all | solution.py:41
  147.9 9.9 %all-to-all-done = f32[32,1,4,128]{3,2,1,0:T(4,128)S(1)} async-done(((f32[32,1,4,128]{3,2,1,0:T(4,128)}), f32[32,1,4,128]{3,2,1,0:T(4,128)S(1)}, u32[]{:S(2)}, u32[]{:S(2)}) %all-to-all-start) | async-done | bytes 65568 | tf_op jit(solution)/shard_map/all_to_all | solution.py:41
  158.0 12.9 %all_to_all.10 = f32[32,1,128]{2,1,0:T(1,128)S(1)} all-to-all(f32[32,1,128]{2,1,0:T(1,128)S(1)} %broadcast_in_dim.21), channel_id=1, replica_groups=mesh['sp_0'=8,'sp_1'=4,'tp'=16] {'sp_0','sp_1'}, dimensions={0} | all-to-all | bytes 32768 | tf_op jit(solution)/shard_map/all_to_all | solution.py:47
  170.9 0.6 multiply_reduce_fusion.1
  172.2 0.5 multiply_bitcast_fusion
  (49 shorter events, 2.5 us)
Async XLA Ops:
  7.2 63.3 %copy-start = (bf16[4096,128]{1,0:T(8,128)(2,1)S(1)}, bf16[4096,128]{1,0:T(8,128)(2,1)}, u32[]{:S(2)}) copy-start(bf16[4096,128]{1,0:T(8,128)(2,1)} %param.13) | copy-start | bytes 3145732
  7.2 62.7 %copy-start.3 = (f32[1,512]{1,0:T(1,128)S(1)}, f32[1,512]{1,0:T(1,128)}, u32[]{:S(2)}) copy-start(f32[1,512]{1,0:T(1,128)} %param.19) | copy-start | bytes 6148
  7.2 58.5 %all-gather.4.cloned.1.call-start = ((), (), s32[]{:S(2)}) async-start(), calls=%async_computation.2 | async-start | bytes 4456448 | tf_op jit(solution)/shard_map/all_gather | solution.py:114
  65.7 8.4 %copy-start.5 = (bf16[4096,128]{1,0:T(8,128)(2,1)S(1)}, bf16[4096,128]{1,0:T(8,128)(2,1)}, u32[]{:S(2)}) copy-start(bf16[4096,128]{1,0:T(8,128)(2,1)} %param.14) | copy-start | bytes 3145732
  70.2 3.9 %copy-start.1 = (bf16[512,4096]{1,0:T(8,128)(2,1)S(1)}, bf16[512,4096]{1,0:T(8,128)(2,1)}, u32[]{:S(2)}) copy-start(bf16[512,4096]{1,0:T(8,128)(2,1)} %all-gather.4.cloned.1.call-done) | copy-start | bytes 12582916
  81.4 66.5 %copy-start.6 = (bf16[1,4]{1,0:T(2,128)(2,1)S(1)}, bf16[1,4]{1,0:T(2,128)(2,1)}, u32[]{:S(2)}) copy-start(bf16[1,4]{1,0:T(2,128)(2,1)} %param.20) | copy-start | bytes 28
  81.4 90.8 %copy-start.4 = (bf16[128]{0:T(256)(128)(2,1)S(1)}, bf16[128]{0:T(256)(128)(2,1)}, u32[]{:S(2)}) copy-start(bf16[128]{0:T(256)(128)(2,1)} %param.21) | copy-start | bytes 772
  140.0 17.9 %all-to-all-start = ((f32[32,1,4,128]{3,2,1,0:T(4,128)}), f32[32,1,4,128]{3,2,1,0:T(4,128)S(1)}, u32[]{:S(2)}, u32[]{:S(2)}) async-start(f32[32,1,4,128]{3,2,1,0:T(4,128)} %copy.34), calls=%async_computation | async-start | bytes 131072 | tf_op jit(solution)/shard_map/all_to_all | solution.py:41
  157.9 14.8 %copy-start.2 = (bf16[4,128]{1,0:T(4,128)(2,1)}, bf16[4,128]{1,0:T(4,128)(2,1)S(1)}, u32[]{:S(2)}) copy-start(bf16[4,128]{1,0:T(4,128)(2,1)S(1)} %reduce_sum.46) | copy-start | bytes 3076
Sparse Core Ops, SparseCore 0:
  10.0 55.5 all-gather.3
where the time goes:
time: 180 us
  waiting for transfers between devices  64.2 us (36%)
  blocking collectives  53 us (29%)
  matrix products  26.5 us (15%)
  between operations  15.8 us (9%)
  local copies, waits for them, and re-layouts  9.17 us (5%)
  starting transfers between devices  7.96 us (4%)
  other arithmetic  2.73 us (2%)
    all_gather x1, waiting for transfers between devices, per_device(): piece = lax.all_gather(tokens, 'tp', axis=1, tiled=True)  53.6 us
    all_gather x2, blocking collectives, entering(): pieces = lax.all_gather(running, axis)  40.2 us
    all_to_all x1, blocking collectives, from_everyone(): lax.all_to_all(jnp.broadcast_to(x[None], (count, *x.shape)), axis, 0, 0,...  12.9 us
    all_to_all x1, waiting for transfers between devices, summed_on_arrival(): lax.all_to_all(pieces, axis, split_axis=0, concat_axis=0, tiled=True)  9.95 us
    dot_general x8, matrix products, advance(): jnp.einsum('hcd,hce->hde', key_remainder, fresh, precision=lax.Precision....  8.06 us
    all_to_all x1, starting transfers between devices, summed_on_arrival(): lax.all_to_all(pieces, axis, split_axis=0, concat_axis=0, tiled=True)  7.92 us
    dot_general x13, matrix products, matmul_f32(): return jnp.dot(left, right, precision=lax.Precision.HIGHEST)  5.5 us
    dynamic_slice x8, local copies, waits for them, and re-layouts, per_device(): lax.scan(advance, jnp.concatenate([value_zeros, identity], axis=-1), inputs)  4.68 us
  transfers between devices with their start and end apart: 2, of which 2 were waited for; matrix products, arithmetic and copies ran while one was open for 2% of the time, Pallas kernels for 0%

commit v1 on v0

--- a/solution.py
+++ b/solution.py
@@ -9,6 +9,12 @@
 BLOCK = 64
 SP = ("sp_0", "sp_1")
 norm_eps = 1e-06
+
+
+def laid_out(blocks, dim):
+    blocks = jnp.moveaxis(blocks, 0, dim)
+    dims = blocks.shape
+    return blocks.reshape(*dims[:dim], dims[dim] * dims[dim + 1], *dims[dim + 2 :])
 
 
 def neutral_like(x, identity):
@@ -111,7 +117,19 @@
         ],
         axis=1,
     )
-    piece = lax.all_gather(tokens, "tp", axis=1, tiled=True)
+    size = lax.axis_size("tp")
+    pairs = [(i, (i + 1) % size) for i in range(size)]
+    back = [(b, a) for a, b in pairs]
+    lower_2, upper = ([], [])
+    for step in range(size - 1):
+        if step % 2 == 0:
+            lower_2.append(lax.ppermute(lower_2[-1] if lower_2 else tokens, "tp", pairs))
+        else:
+            upper.append(lax.ppermute(upper[-1] if upper else tokens, "tp", back))
+    pieces_2 = jnp.stack([*lower_2[::-1], tokens, *upper])
+    shift = lax.axis_index("tp") - len(lower_2)
+    pieces_2 = pieces_2[(jnp.arange(size) - shift) % size]
+    piece = laid_out(pieces_2, 1)
     key_acc = jnp.dot(piece, w_key, preferred_element_type=jnp.float32)
     value_acc = jnp.dot(piece, w_value, preferred_element_type=jnp.float32)
     gate_acc = jnp.dot(piece, gate_weights, preferred_element_type=jnp.float32)

time: 180 us -> 195 us (1.083)
  the two profiles are of different devices: /device:TPU:8 before, /device:TPU:32 now
where the time goes in v1:
time: 195 us
  blocking collectives  57.6 us (30%)
  waiting for transfers between devices  40.8 us (21%)
  local copies, waits for them, and re-layouts  38.5 us (20%)
  starting transfers between devices  27.4 us (14%)
  matrix products  25 us (13%)
  other arithmetic  2.67 us (1%)
  between operations  2.46 us (1%)
    all_gather x2, blocking collectives, entering(): pieces = lax.all_gather(running, axis)  44.8 us
    ppermute x8, waiting for transfers between devices, per_device(): lax.ppermute(lower_2[-1] if lower_2 else tokens, 'tp', pairs)  29.4 us
    ppermute x7, starting transfers between devices, per_device(): upper.append(lax.ppermute(upper[-1] if upper else tokens, 'tp', back))  21.3 us
    unnamed x37, local copies, waits for them, and re-layouts  17.2 us
    all_to_all x1, blocking collectives, from_everyone(): lax.all_to_all(jnp.broadcast_to(x[None], (count, *x.shape)), axis, 0, 0,...  12.9 us
    all_to_all x1, waiting for transfers between devices, summed_on_arrival(): lax.all_to_all(pieces, axis, split_axis=0, concat_axis=0, tiled=True)  9.95 us
    dot_general x8, matrix products, advance(): jnp.einsum('hcd,hce->hde', key_remainder, fresh, precision=lax.Precision....  8.04 us
    transpose x1, local copies, waits for them, and re-layouts, laid_out(): blocks = jnp.moveaxis(blocks, 0, dim)  6.41 us
  transfers between devices with their start and end apart: 16, of which 11 were waited for; matrix products, arithmetic and copies ran while one was open for 10% of the time, Pallas kernels for 0%

profile of v1, /device:TPU:32, one launch (start us, length us, event | category | flops | bytes accessed | tf_op | source)
XLA Modules:
  0.0 194.7 jit_solution(6173698594218950476)
XLA Ops:
  0.7 7.2 %collective-permute-done = bf16[512,256]{1,0:T(8,128)(2,1)S(1)} collective-permute-done((bf16[512,256]{1,0:T(8,128)(2,1)}, bf16[512,256]{1,0:T(8,128)(2,1)S(1)}, u32[]{:S(2)}, u32[]{:S(2)}) %collective-permute-start) | collective-permute-done | bytes 262176 | tf_op jit(solution)/shard_map/ppermute | solution.py:126
  7.9 3.0 %collective-permute-start.8 = (bf16[512,256]{1,0:T(8,128)(2,1)}, bf16[512,256]{1,0:T(8,128)(2,1)S(1)}, u32[]{:S(2)}, u32[]{:S(2)}) collective-permute-start(bf16[512,256]{1,0:T(8,128)(2,1)} %param.12), channel_id=1, source_target_pairs={{1,0},{2,1},{3,2},{4,3},{5,4},{6,5},{7,6},{8,7},{9,8},{10,9},{11,1... | collective-permute-start | bytes 786440 | tf_op jit(solution)/shard_map/ppermute | solution.py:128
  10.9 4.1 %collective-permute-done.1 = bf16[512,256]{1,0:T(8,128)(2,1)S(1)} collective-permute-done((bf16[512,256]{1,0:T(8,128)(2,1)S(1)}, bf16[512,256]{1,0:T(8,128)(2,1)S(1)}, u32[]{:S(2)}, u32[]{:S(2)}) %collective-permute-start.1) | collective-permute-done | bytes 262176 | tf_op jit(solution)/shard_map/ppermute | solution.py:126
  15.1 3.0 %collective-permute-start.9 = (bf16[512,256]{1,0:T(8,128)(2,1)S(1)}, bf16[512,256]{1,0:T(8,128)(2,1)S(1)}, u32[]{:S(2)}, u32[]{:S(2)}) collective-permute-start(bf16[512,256]{1,0:T(8,128)(2,1)S(1)} %collective-permute-done.8), channel_id=1, source_target_pairs={{1,0},{2,1},{3,2},{4,3},{5,4},{6,5},{7,6},{8,7},{9,8},{10,9},{11,1... | collective-permute-start | bytes 786440 | tf_op jit(solution)/shard_map/ppermute | solution.py:128
  18.1 3.8 %collective-permute-done.2 = bf16[512,256]{1,0:T(8,128)(2,1)S(1)} collective-permute-done((bf16[512,256]{1,0:T(8,128)(2,1)S(1)}, bf16[512,256]{1,0:T(8,128)(2,1)S(1)}, u32[]{:S(2)}, u32[]{:S(2)}) %collective-permute-start.2) | collective-permute-done | bytes 262176 | tf_op jit(solution)/shard_map/ppermute | solution.py:126
  22.0 3.1 %collective-permute-start.10 = (bf16[512,256]{1,0:T(8,128)(2,1)S(1)}, bf16[512,256]{1,0:T(8,128)(2,1)S(1)}, u32[]{:S(2)}, u32[]{:S(2)}) collective-permute-start(bf16[512,256]{1,0:T(8,128)(2,1)S(1)} %collective-permute-done.9), channel_id=1, source_target_pairs={{1,0},{2,1},{3,2},{4,3},{5,4},{6,5},{7,6},{8,7},{9,8},{10,9},{11,1... | collective-permute-start | bytes 786440 | tf_op jit(solution)/shard_map/ppermute | solution.py:128
  25.1 3.8 %collective-permute-done.3 = bf16[512,256]{1,0:T(8,128)(2,1)S(1)} collective-permute-done((bf16[512,256]{1,0:T(8,128)(2,1)S(1)}, bf16[512,256]{1,0:T(8,128)(2,1)S(1)}, u32[]{:S(2)}, u32[]{:S(2)}) %collective-permute-start.3) | collective-permute-done | bytes 262176 | tf_op jit(solution)/shard_map/ppermute | solution.py:126
  29.0 3.1 %collective-permute-start.11 = (bf16[512,256]{1,0:T(8,128)(2,1)S(1)}, bf16[512,256]{1,0:T(8,128)(2,1)S(1)}, u32[]{:S(2)}, u32[]{:S(2)}) collective-permute-start(bf16[512,256]{1,0:T(8,128)(2,1)S(1)} %collective-permute-done.10), channel_id=1, source_target_pairs={{1,0},{2,1},{3,2},{4,3},{5,4},{6,5},{7,6},{8,7},{9,8},{10,9},{11,1... | collective-permute-start | bytes 786440 | tf_op jit(solution)/shard_map/ppermute | solution.py:128
  32.1 3.9 %collective-permute-done.4 = bf16[512,256]{1,0:T(8,128)(2,1)} collective-permute-done((bf16[512,256]{1,0:T(8,128)(2,1)S(1)}, bf16[512,256]{1,0:T(8,128)(2,1)}, u32[]{:S(2)}, u32[]{:S(2)}) %collective-permute-start.4) | collective-permute-done | bytes 262176 | tf_op jit(solution)/shard_map/ppermute | solution.py:126
  36.1 0.9 constant_dynamic-slice_fusion.1
  37.0 0.7 copy-done.4
  37.7 3.0 %collective-permute-start.12 = (bf16[512,256]{1,0:T(8,128)(2,1)S(1)}, bf16[512,256]{1,0:T(8,128)(2,1)}, u32[]{:S(2)}, u32[]{:S(2)}) collective-permute-start(bf16[512,256]{1,0:T(8,128)(2,1)S(1)} %collective-permute-done.11), channel_id=1, source_target_pairs={{1,0},{2,1},{3,2},{4,3},{5,4},{6,5},{7,6},{8,7},{9,8},{10,9},{11,1... | collective-permute-start | bytes 786440 | tf_op jit(solution)/shard_map/ppermute | solution.py:128
  40.7 2.6 %collective-permute-done.5 = bf16[512,256]{1,0:T(8,128)(2,1)S(1)} collective-permute-done((bf16[512,256]{1,0:T(8,128)(2,1)}, bf16[512,256]{1,0:T(8,128)(2,1)S(1)}, u32[]{:S(2)}, u32[]{:S(2)}) %collective-permute-start.5) | collective-permute-done | bytes 262176 | tf_op jit(solution)/shard_map/ppermute | solution.py:126
  43.4 1.2 collective-permute-done.12
  44.5 3.2 %collective-permute-start.13 = (bf16[512,256]{1,0:T(8,128)(2,1)}, bf16[512,256]{1,0:T(8,128)(2,1)}, u32[]{:S(2)}, u32[]{:S(2)}) collective-permute-start(bf16[512,256]{1,0:T(8,128)(2,1)} %collective-permute-done.12), channel_id=1, source_target_pairs={{1,0},{2,1},{3,2},{4,3},{5,4},{6,5},{7,6},{8,7},{9,8},{10,9},{11,1... | collective-permute-start | bytes 786440 | tf_op jit(solution)/shard_map/ppermute | solution.py:128
  47.8 2.6 %collective-permute-done.6 = bf16[512,256]{1,0:T(8,128)(2,1)} collective-permute-done((bf16[512,256]{1,0:T(8,128)(2,1)S(1)}, bf16[512,256]{1,0:T(8,128)(2,1)}, u32[]{:S(2)}, u32[]{:S(2)}) %collective-permute-start.6) | collective-permute-done | bytes 262176 | tf_op jit(solution)/shard_map/ppermute | solution.py:126
  50.4 1.2 dynamic_slice.29
  51.6 1.2 dynamic_slice.26
  53.6 2.9 %collective-permute-start.14 = (bf16[512,256]{1,0:T(8,128)(2,1)}, bf16[512,256]{1,0:T(8,128)(2,1)S(1)}, u32[]{:S(2)}, u32[]{:S(2)}) collective-permute-start(bf16[512,256]{1,0:T(8,128)(2,1)} %collective-permute-done.13), channel_id=1, source_target_pairs={{1,0},{2,1},{3,2},{4,3},{5,4},{6,5},{7,6},{8,7},{9,8},{10,9},{11,1... | collective-permute-start | bytes 786440 | tf_op jit(solution)/shard_map/ppermute | solution.py:128
  56.5 1.2 collective-permute-done.7
  57.7 1.7 bitcast_dynamic-update-slice_fusion.15
  59.4 1.7 bitcast_dynamic-update-slice_fusion.14
  61.0 1.7 bitcast_dynamic-update-slice_fusion.13
  62.7 1.7 bitcast_dynamic-update-slice_fusion.12
  64.4 0.7 bitcast_dynamic-update-slice_fusion.11
  65.1 0.7 bitcast_dynamic-update-slice_fusion.10
  65.8 0.7 bitcast_dynamic-update-slice_fusion.9
  66.5 0.7 bitcast_dynamic-update-slice_fusion.8
  67.3 0.7 bitcast_dynamic-update-slice_fusion.7
  68.0 0.7 bitcast_dynamic-update-slice_fusion.6
  68.7 0.7 bitcast_dynamic-update-slice_fusion.5
  69.4 0.7 bitcast_dynamic-update-slice_fusion.4
  70.2 0.7 bitcast_dynamic-update-slice_fusion.3
  70.9 1.7 bitcast_dynamic-update-slice_fusion.2
  72.6 1.7 bitcast_dynamic-update-slice_fusion.1
  74.2 0.7 bitcast_dynamic-update-slice_fusion
  74.9 5.0 %gather_fusion = bf16[16,512,256]{2,1,0:T(8,128)(2,1)} fusion(bf16[16,512,256]{2,1,0:T(8,128)(2,1)} %bitcast_dynamic-update-slice_fusion, s32[1024]{0:T(1024)S(1)} %pad_clamp_fusion), kind=kCustom, calls=%fused_computation | custom fusion | bytes 8388672 | tf_op jit(solution)/shard_map/gather | solution.py:131
  79.9 6.4 %copy.37 = bf16[512,16,256]{0,2,1:T(8,128)(2,1)} copy(bf16[512,16,256]{2,0,1:T(8,128)(2,1)} %bitcast.172) | data formatting | bytes 8388608 | tf_op jit(solution)/shard_map/transpose | solution.py:15
  86.3 3.6 %convolution_convert_fusion.1 = bf16[512,128]{1,0:T(8,128)(2,1)S(1)} fusion(bf16[512,4096]{0,1:T(8,128)(2,1)} %bitcast.169, bf16[4096,128]{1,0:T(8,128)(2,1)S(1)} %copy-done), kind=kOutput, calls=%fused_computation.21 | convolution fusion | flops 536936448 | bytes 5373952 | tf_op jit(solution)/shard_map/dot_general | solution.py:133
  90.3 0.6 fusion.68
  92.1 0.6 fusion.10
  96.3 2.5 %convolution_convert_fusion = bf16[512,128]{1,0:T(8,128)(2,1)S(1)} fusion(bf16[512,4096]{0,1:T(8,128)(2,1)S(1)} %bitcast.171, bf16[4096,128]{1,0:T(8,128)(2,1)} %param.14), kind=kOutput, calls=%fused_computation.20 | convolution fusion | flops 536936448 | bytes 5373952 | tf_op jit(solution)/shard_map/dot_general | solution.py:134
  100.5 14.8 %while.10 = (s32[]{:T(128)}, f32[1,128,256]{2,1,0:T(8,128)S(1)}, f32[8,1]{0,1:T(1,128)S(1)}, f32[8,1,64,128]{3,2,1,0:T(8,128)S(1)}, f32[8,1,64,128]{3,2,1,0:T(8,...) while((s32[]{:T(128)}, f32[1,128,256]{2,1,0:T(8,128)S(1)}, f32[8,1]{0,1:T(1,128)S(1)}, ...), condition=%wide.region_3.4_spmd, body=%wide.region_2.3_spmd.sunk | while | flops 50413568 | bytes 688233 | solution.py:177
  100.7 0.6 constant_dynamic-slice_fusion.4
  101.3 1.0 fusion.136
  102.6 0.6 constant_dynamic-slice_fusion.4
  103.2 1.0 fusion.136
  104.4 0.6 constant_dynamic-slice_fusion.4
  105.0 1.0 fusion.136
  106.3 0.6 constant_dynamic-slice_fusion.4
  106.9 1.0 fusion.136
  108.1 0.6 constant_dynamic-slice_fusion.4
  108.7 1.0 fusion.136
  110.0 0.6 constant_dynamic-slice_fusion.4
  110.5 1.0 fusion.136
  112.4 1.0 fusion.136
  114.2 1.0 fusion.136
  115.3 12.7 %all-gather = f32[4,128,128]{2,1,0:T(8,128)S(1)} all-gather(f32[1,128,128]{2,1,0:T(8,128)S(1)} %slice.55), channel_id=2, replica_groups=mesh['sp_0'=8,'sp_1'=4,'tp'=16] {'sp_1'}, dimensions={0}, use_global_device_ids=true | all-gather | bytes 327680 | tf_op jit(solution)/shard_map/all_gather | solution.py:29
  128.8 32.0 %all-gather.1 = f32[1024,128]{1,0:T(8,128)S(1)} all-gather(f32[128,128]{1,0:T(8,128)S(1)} %fusion.56), channel_id=3, replica_groups=mesh['sp_0'=8,'sp_1'=4,'tp'=16] {'sp_0'}, dimensions={0}, use_global_device_ids=true | all-gather | bytes 589824 | tf_op jit(solution)/shard_map/all_gather | solution.py:29
  163.2 0.7 copy.42
  163.8 6.0 %all-to-all-start = ((f32[32,1,4,128]{3,2,1,0:T(4,128)}), f32[32,1,4,128]{3,2,1,0:T(4,128)S(1)}, u32[]{:S(2)}, u32[]{:S(2)}) async-start(f32[32,1,4,128]{3,2,1,0:T(4,128)} %copy.42), calls=%async_computation | async-start | bytes 131072 | tf_op jit(solution)/shard_map/all_to_all | solution.py:47
  169.9 9.9 %all-to-all-done = f32[32,1,4,128]{3,2,1,0:T(4,128)S(1)} async-done(((f32[32,1,4,128]{3,2,1,0:T(4,128)}), f32[32,1,4,128]{3,2,1,0:T(4,128)S(1)}, u32[]{:S(2)}, u32[]{:S(2)}) %all-to-all-start) | async-done | bytes 65568 | tf_op jit(solution)/shard_map/all_to_all | solution.py:47
  179.9 12.9 %all_to_all.10 = f32[32,1,128]{2,1,0:T(1,128)S(1)} all-to-all(f32[32,1,128]{2,1,0:T(1,128)S(1)} %broadcast_in_dim.21), channel_id=1, replica_groups=mesh['sp_0'=8,'sp_1'=4,'tp'=16] {'sp_0','sp_1'}, dimensions={0} | all-to-all | bytes 32768 | tf_op jit(solution)/shard_map/all_to_all | solution.py:53
  192.8 0.6 multiply_reduce_fusion.1
  (104 shorter events, 13.5 us)
Async XLA Ops:
  0.6 85.7 %copy-start = (bf16[4096,128]{1,0:T(8,128)(2,1)S(1)}, bf16[4096,128]{1,0:T(8,128)(2,1)}, u32[]{:S(2)}) copy-start(bf16[4096,128]{1,0:T(8,128)(2,1)} %param.13) | copy-start | bytes 3145732
  0.6 66.6 %copy-start.3 = (bf16[512,256]{1,0:T(8,128)(2,1)S(1)}, bf16[512,256]{1,0:T(8,128)(2,1)}, u32[]{:S(2)}) copy-start(bf16[512,256]{1,0:T(8,128)(2,1)} %param.12) | copy-start | bytes 786436
  0.7 7.3 %collective-permute-start = (bf16[512,256]{1,0:T(8,128)(2,1)}, bf16[512,256]{1,0:T(8,128)(2,1)S(1)}, u32[]{:S(2)}, u32[]{:S(2)}) collective-permute-start(bf16[512,256]{1,0:T(8,128)(2,1)} %param.12), channel_id=1, source_target_pairs={{0,1},{1,2},{2,3},{3,4},{4,5},{5,6},{6,7},{7,8},{8,9},{9,10},{10,1... | collective-permute-start | bytes 786440 | tf_op jit(solution)/shard_map/ppermute | solution.py:126
  7.9 7.0 %collective-permute-start.1 = (bf16[512,256]{1,0:T(8,128)(2,1)S(1)}, bf16[512,256]{1,0:T(8,128)(2,1)S(1)}, u32[]{:S(2)}, u32[]{:S(2)}) collective-permute-start(bf16[512,256]{1,0:T(8,128)(2,1)S(1)} %collective-permute-done), channel_id=1, source_target_pairs={{0,1},{1,2},{2,3},{3,4},{4,5},{5,6},{6,7},{7,8},{8,9},{9,10},{10,1... | collective-permute-start | bytes 786440 | tf_op jit(solution)/shard_map/ppermute | solution.py:126
  7.9 7.2 %collective-permute-start.8 = (bf16[512,256]{1,0:T(8,128)(2,1)}, bf16[512,256]{1,0:T(8,128)(2,1)S(1)}, u32[]{:S(2)}, u32[]{:S(2)}) collective-permute-start(bf16[512,256]{1,0:T(8,128)(2,1)} %param.12), channel_id=1, source_target_pairs={{1,0},{2,1},{3,2},{4,3},{5,4},{6,5},{7,6},{8,7},{9,8},{10,9},{11,1... | collective-permute-start | bytes 786440 | tf_op jit(solution)/shard_map/ppermute | solution.py:128
  14.9 7.0 %collective-permute-start.2 = (bf16[512,256]{1,0:T(8,128)(2,1)S(1)}, bf16[512,256]{1,0:T(8,128)(2,1)S(1)}, u32[]{:S(2)}, u32[]{:S(2)}) collective-permute-start(bf16[512,256]{1,0:T(8,128)(2,1)S(1)} %collective-permute-done.1), channel_id=1, source_target_pairs={{0,1},{1,2},{2,3},{3,4},{4,5},{5,6},{6,7},{7,8},{8,9},{9,10},{10,1... | collective-permute-start | bytes 786440 | tf_op jit(solution)/shard_map/ppermute | solution.py:126
  15.1 6.9 %collective-permute-start.9 = (bf16[512,256]{1,0:T(8,128)(2,1)S(1)}, bf16[512,256]{1,0:T(8,128)(2,1)S(1)}, u32[]{:S(2)}, u32[]{:S(2)}) collective-permute-start(bf16[512,256]{1,0:T(8,128)(2,1)S(1)} %collective-permute-done.8), channel_id=1, source_target_pairs={{1,0},{2,1},{3,2},{4,3},{5,4},{6,5},{7,6},{8,7},{9,8},{10,9},{11,1... | collective-permute-start | bytes 786440 | tf_op jit(solution)/shard_map/ppermute | solution.py:128
  21.9 7.0 %collective-permute-start.3 = (bf16[512,256]{1,0:T(8,128)(2,1)S(1)}, bf16[512,256]{1,0:T(8,128)(2,1)S(1)}, u32[]{:S(2)}, u32[]{:S(2)}) collective-permute-start(bf16[512,256]{1,0:T(8,128)(2,1)S(1)} %collective-permute-done.2), channel_id=1, source_target_pairs={{0,1},{1,2},{2,3},{3,4},{4,5},{5,6},{6,7},{7,8},{8,9},{9,10},{10,1... | collective-permute-start | bytes 786440 | tf_op jit(solution)/shard_map/ppermute | solution.py:126
  22.0 7.0 %collective-permute-start.10 = (bf16[512,256]{1,0:T(8,128)(2,1)S(1)}, bf16[512,256]{1,0:T(8,128)(2,1)S(1)}, u32[]{:S(2)}, u32[]{:S(2)}) collective-permute-start(bf16[512,256]{1,0:T(8,128)(2,1)S(1)} %collective-permute-done.9), channel_id=1, source_target_pairs={{1,0},{2,1},{3,2},{4,3},{5,4},{6,5},{7,6},{8,7},{9,8},{10,9},{11,1... | collective-permute-start | bytes 786440 | tf_op jit(solution)/shard_map/ppermute | solution.py:128
  29.0 7.1 %collective-permute-start.4 = (bf16[512,256]{1,0:T(8,128)(2,1)S(1)}, bf16[512,256]{1,0:T(8,128)(2,1)}, u32[]{:S(2)}, u32[]{:S(2)}) collective-permute-start(bf16[512,256]{1,0:T(8,128)(2,1)S(1)} %collective-permute-done.3), channel_id=1, source_target_pairs={{0,1},{1,2},{2,3},{3,4},{4,5},{5,6},{6,7},{7,8},{8,9},{9,10},{10,1... | collective-permute-start | bytes 786440 | tf_op jit(solution)/shard_map/ppermute | solution.py:126
  29.0 8.0 %collective-permute-start.11 = (bf16[512,256]{1,0:T(8,128)(2,1)S(1)}, bf16[512,256]{1,0:T(8,128)(2,1)S(1)}, u32[]{:S(2)}, u32[]{:S(2)}) collective-permute-start(bf16[512,256]{1,0:T(8,128)(2,1)S(1)} %collective-permute-done.10), channel_id=1, source_target_pairs={{1,0},{2,1},{3,2},{4,3},{5,4},{6,5},{7,6},{8,7},{9,8},{10,9},{11,1... | collective-permute-start | bytes 786440 | tf_op jit(solution)/shard_map/ppermute | solution.py:128
  36.1 7.2 %collective-permute-start.5 = (bf16[512,256]{1,0:T(8,128)(2,1)}, bf16[512,256]{1,0:T(8,128)(2,1)S(1)}, u32[]{:S(2)}, u32[]{:S(2)}) collective-permute-start(bf16[512,256]{1,0:T(8,128)(2,1)} %collective-permute-done.4), channel_id=1, source_target_pairs={{0,1},{1,2},{2,3},{3,4},{4,5},{5,6},{6,7},{7,8},{8,9},{9,10},{10,1... | collective-permute-start | bytes 786440 | tf_op jit(solution)/shard_map/ppermute | solution.py:126
  37.0 0.7 copy-start.4
  37.7 6.8 %collective-permute-start.12 = (bf16[512,256]{1,0:T(8,128)(2,1)S(1)}, bf16[512,256]{1,0:T(8,128)(2,1)}, u32[]{:S(2)}, u32[]{:S(2)}) collective-permute-start(bf16[512,256]{1,0:T(8,128)(2,1)S(1)} %collective-permute-done.11), channel_id=1, source_target_pairs={{1,0},{2,1},{3,2},{4,3},{5,4},{6,5},{7,6},{8,7},{9,8},{10,9},{11,1... | collective-permute-start | bytes 786440 | tf_op jit(solution)/shard_map/ppermute | solution.py:128
  43.3 1.3 copy-start.6
  43.3 7.1 %collective-permute-start.6 = (bf16[512,256]{1,0:T(8,128)(2,1)S(1)}, bf16[512,256]{1,0:T(8,128)(2,1)}, u32[]{:S(2)}, u32[]{:S(2)}) collective-permute-start(bf16[512,256]{1,0:T(8,128)(2,1)S(1)} %collective-permute-done.5), channel_id=1, source_target_pairs={{0,1},{1,2},{2,3},{3,4},{4,5},{5,6},{6,7},{7,8},{8,9},{9,10},{10,1... | collective-permute-start | bytes 786440 | tf_op jit(solution)/shard_map/ppermute | solution.py:126
  44.5 9.0 %collective-permute-start.13 = (bf16[512,256]{1,0:T(8,128)(2,1)}, bf16[512,256]{1,0:T(8,128)(2,1)}, u32[]{:S(2)}, u32[]{:S(2)}) collective-permute-start(bf16[512,256]{1,0:T(8,128)(2,1)} %collective-permute-done.12), channel_id=1, source_target_pairs={{1,0},{2,1},{3,2},{4,3},{5,4},{6,5},{7,6},{8,7},{9,8},{10,9},{11,1... | collective-permute-start | bytes 786440 | tf_op jit(solution)/shard_map/ppermute | solution.py:128
  50.4 7.3 %collective-permute-start.7 = (bf16[512,256]{1,0:T(8,128)(2,1)}, bf16[512,256]{1,0:T(8,128)(2,1)}, u32[]{:S(2)}, u32[]{:S(2)}) collective-permute-start(bf16[512,256]{1,0:T(8,128)(2,1)} %collective-permute-done.6), channel_id=1, source_target_pairs={{0,1},{1,2},{2,3},{3,4},{4,5},{5,6},{6,7},{7,8},{8,9},{9,10},{10,1... | collective-permute-start | bytes 786440 | tf_op jit(solution)/shard_map/ppermute | solution.py:126
  53.5 16.6 %copy-start.5 = (bf16[512,256]{1,0:T(8,128)(2,1)S(1)}, bf16[512,256]{1,0:T(8,128)(2,1)}, u32[]{:S(2)}) copy-start(bf16[512,256]{1,0:T(8,128)(2,1)} %copy-done.4) | copy-start | bytes 786436
  53.6 20.6 %collective-permute-start.14 = (bf16[512,256]{1,0:T(8,128)(2,1)}, bf16[512,256]{1,0:T(8,128)(2,1)S(1)}, u32[]{:S(2)}, u32[]{:S(2)}) collective-permute-start(bf16[512,256]{1,0:T(8,128)(2,1)} %collective-permute-done.13), channel_id=1, source_target_pairs={{1,0},{2,1},{3,2},{4,3},{5,4},{6,5},{7,6},{8,7},{9,8},{10,9},{11,1... | collective-permute-start | bytes 786440 | tf_op jit(solution)/shard_map/ppermute | solution.py:128
  86.3 4.0 %copy-start.1 = (bf16[512,16,256]{0,2,1:T(8,128)(2,1)S(1)}, bf16[512,16,256]{0,2,1:T(8,128)(2,1)}, u32[]{:S(2)}) copy-start(bf16[512,16,256]{0,2,1:T(8,128)(2,1)} %copy.37) | copy-start | bytes 12582916
  86.3 5.3 %copy-start.8 = (f32[1,512]{1,0:T(1,128)S(1)}, f32[1,512]{1,0:T(1,128)}, u32[]{:S(2)}) copy-start(f32[1,512]{1,0:T(1,128)} %param.19) | copy-start | bytes 6148
  91.9 4.4 %copy-start.2 = (bf16[512,16,256]{0,2,1:T(8,128)(2,1)S(1)}, bf16[512,16,256]{0,2,1:T(8,128)(2,1)}, u32[]{:S(2)}) copy-start(bf16[512,16,256]{0,2,1:T(8,128)(2,1)} %copy.37) | copy-start | bytes 12582916
  100.5 69.4 %copy-start.10 = (bf16[1,4]{1,0:T(2,128)(2,1)S(1)}, bf16[1,4]{1,0:T(2,128)(2,1)}, u32[]{:S(2)}) copy-start(bf16[1,4]{1,0:T(2,128)(2,1)} %param.20) | copy-start | bytes 28
  100.5 93.7 %copy-start.9 = (bf16[128]{0:T(256)(128)(2,1)S(1)}, bf16[128]{0:T(256)(128)(2,1)}, u32[]{:S(2)}) copy-start(bf16[128]{0:T(256)(128)(2,1)} %param.21) | copy-start | bytes 772
  163.8 16.0 %all-to-all-start = ((f32[32,1,4,128]{3,2,1,0:T(4,128)}), f32[32,1,4,128]{3,2,1,0:T(4,128)S(1)}, u32[]{:S(2)}, u32[]{:S(2)}) async-start(f32[32,1,4,128]{3,2,1,0:T(4,128)} %copy.42), calls=%async_computation | async-start | bytes 131072 | tf_op jit(solution)/shard_map/all_to_all | solution.py:47
  179.8 14.8 %copy-start.7 = (bf16[4,128]{1,0:T(4,128)(2,1)}, bf16[4,128]{1,0:T(4,128)(2,1)S(1)}, u32[]{:S(2)}) copy-start(bf16[4,128]{1,0:T(4,128)(2,1)S(1)} %reduce_sum.46) | copy-start | bytes 3076
